TPU v7x, 32 devices: a whole 2x2x4 slice. The times are simulated.
32 devices in a mesh: sp: 4 (over z), tp: 8 (over y, x, core).
Axes of the slice: x: 2, y: 2, z: 4, core: 2. Of those that a mesh axis runs over, the one named last changes fastest.
Arguments:
- tokens: bfloat16 [3072, 2048], P('sp'), may hold values from -6 to 6
- norm_gain: float32 [2048], replicated, may hold values from 0.5 to 80
- grid_query_weight: bfloat16 [2048, 2048], P(None, 'tp'), may hold values from -0.5 to 0.5
- grid_key_weight: bfloat16 [2048, 1024], P(None, 'tp'), may hold values from -0.5 to 0.5
- grid_value_weight: bfloat16 [2048, 1024], P(None, 'tp'), may hold values from -0.5 to 0.5
- grid_query_gain: float32 [128], replicated, may hold values from 1.6 to 6
- grid_key_gain: float32 [128], replicated, may hold values from 1.6 to 6
- local_query_weight: bfloat16 [2048, 2048], P(None, 'tp'), may hold values from -0.5 to 0.5
- local_key_weight: bfloat16 [2048, 1024], P(None, 'tp'), may hold values from -0.5 to 0.5
- local_value_weight: bfloat16 [2048, 1024], P(None, 'tp'), may hold values from -0.5 to 0.5
- sink_logit: float32 [16], P('tp'), may hold values from 1 to 6
- grid_out_weight: bfloat16 [2048, 2048], P('tp'), may hold values from -0.09375 to 0.09375
- local_out_weight: bfloat16 [2048, 2048], P('tp'), may hold values from -0.09375 to 0.09375
Outputs:
- mixed: bfloat16 [3072, 2048], P(('sp', 'tp'))
All inputs are finite; a program needn't handle non-finite values.
Results may differ from a plain program's by a relative error of at most 0.03.
Values may be sent and summed in bfloat16 or wider, within the bound.
A program may use at most 192 MiB of HBM per device.

v0:
```python
import math

import jax
import jax.numpy as jnp
from jax import lax
from jax.sharding import PartitionSpec as P

HEAD = 128
WINDOW = 128
GRID_W = 64


EPSILON = 1e-06
ROPE_BASE = 10000.0


def padded(block, sides, width):
    for axis, dim in sides:
        count = lax.axis_size(axis)
        forward = [(i, i + 1) for i in range(count - 1)]
        backward = [(target, source) for source, target in forward]
        low = lax.ppermute(
            lax.slice_in_dim(block, block.shape[dim] - width, None, axis=dim), axis, forward
        )
        high = lax.ppermute(lax.slice_in_dim(block, 0, width, axis=dim), axis, backward)
        block = jnp.concatenate([low, block, high], axis=dim)
    return block


def rms_rows(values, gain):
    widened = values.astype(jnp.float32)
    return widened * lax.rsqrt(jnp.mean(widened * widened, axis=-1, keepdims=True) + EPSILON) * gain


def half_turn(part, angles):
    cosine = jnp.cos(angles)
    sine = jnp.sin(angles)
    cosine = jnp.concatenate([cosine, cosine], axis=-1)
    sine = jnp.concatenate([sine, sine], axis=-1)
    first, second = jnp.split(part, 2, axis=-1)
    turned = jnp.concatenate([-second, first], axis=-1)
    return part * cosine + turned * sine


def axial_turn(heads, positions):
    half_dim = heads.shape[-1] // 2
    inverse = ROPE_BASE ** (-jnp.arange(0, half_dim, 2, dtype=jnp.float32) / half_dim)
    row_angle = (positions // GRID_W).astype(jnp.float32)[:, None, None] * inverse
    col_angle = (positions % GRID_W).astype(jnp.float32)[:, None, None] * inverse
    return jnp.concatenate(
        [half_turn(heads[..., :half_dim], row_angle), half_turn(heads[..., half_dim:], col_angle)],
        axis=-1,
    )


def shards(
    tokens,
    norm_gain,
    grid_query_weight,
    grid_key_weight,
    grid_value_weight,
    grid_query_gain,
    grid_key_gain,
    local_query_weight,
    local_key_weight,
    local_value_weight,
    sink_logit,
    grid_out_weight,
    local_out_weight,
):
    row_count = tokens.shape[0]
    seq_devices = lax.axis_size("sp")
    total_rows = row_count * seq_devices
    offset = lax.axis_index("sp") * row_count
    positions = offset + jnp.arange(row_count, dtype=jnp.int32)
    normed = rms_rows(tokens, norm_gain).astype(jnp.bfloat16)
    score_scale = HEAD ** (-0.5)
    width = grid_out_weight.shape[1]

    def project(weight):
        return jnp.dot(normed, weight, preferred_element_type=jnp.float32).astype(jnp.bfloat16)

    grid_heads = grid_query_weight.shape[1] // HEAD
    grid_groups = grid_key_weight.shape[1] // HEAD
    group_size = grid_heads // grid_groups
    queries = (
        axial_turn(
            rms_rows(
                project(grid_query_weight).reshape(row_count, grid_heads, HEAD), grid_query_gain
            ),
            positions,
        )
        .astype(jnp.bfloat16)
        .reshape(row_count, grid_groups, group_size, HEAD)
    )
    keys = axial_turn(
        rms_rows(project(grid_key_weight).reshape(row_count, grid_groups, HEAD), grid_key_gain),
        positions,
    ).astype(jnp.bfloat16)
    values = project(grid_value_weight).reshape(row_count, grid_groups, HEAD)

    def absorb(carry, pieces):
        running, totals, summed = carry
        scores = (
            jnp.einsum("qhgd,shd->hgqs", queries, pieces[0], preferred_element_type=jnp.float32)
            * score_scale
        )
        highest = jnp.maximum(running, jnp.max(scores, axis=-1))
        factor = jnp.exp(running - highest)
        weights = jnp.exp(scores - highest[..., None])
        totals = totals * factor + jnp.sum(weights, axis=-1)
        summed = summed * factor[..., None] + jnp.einsum(
            "hgqs,shd->hgqd",
            weights.astype(jnp.bfloat16),
            pieces[1],
            preferred_element_type=jnp.float32,
        )
        return (highest, totals, summed)

    initial = (
        jnp.full((grid_groups, group_size, row_count), -jnp.inf, jnp.float32),
        jnp.zeros((grid_groups, group_size, row_count), jnp.float32),
        jnp.zeros((grid_groups, group_size, row_count, HEAD), jnp.float32),
    )
    all_keys, all_values = (
        lax.all_gather(keys, "sp", axis=0, tiled=True),
        lax.all_gather(values, "sp", axis=0, tiled=True),
    )
    shards_per_step = math.gcd(seq_devices, max(1, 2048 // row_count))
    step_rows = row_count * shards_per_step

    def visit(index, carry):
        start = index * step_rows
        piece_keys = lax.dynamic_slice_in_dim(all_keys, start, step_rows, 0)
        piece_values = lax.dynamic_slice_in_dim(all_values, start, step_rows, 0)
        return absorb(carry, (piece_keys, piece_values))

    state = lax.fori_loop(0, total_rows // step_rows, visit, initial)
    running, totals, summed = state
    grid_result = jnp.transpose(summed / totals[..., None], (2, 0, 1, 3))
    grid_result = grid_result.reshape(row_count, grid_heads * HEAD).astype(jnp.bfloat16)
    local_heads = local_query_weight.shape[1] // HEAD
    local_groups = local_key_weight.shape[1] // HEAD
    local_size = local_heads // local_groups
    blocks = row_count // WINDOW
    local_queries = project(local_query_weight).reshape(
        blocks, WINDOW, local_groups, local_size, HEAD
    )
    pairs = jnp.stack(
        [
            project(local_key_weight).reshape(row_count, local_groups, HEAD),
            project(local_value_weight).reshape(row_count, local_groups, HEAD),
        ],
        axis=1,
    )
    widened = padded(pairs, (("sp", 0),), WINDOW)
    framed = widened.reshape(blocks + 2, WINDOW, 2, local_groups, HEAD)
    band = jnp.concatenate([framed[:-2], framed[1:-1], framed[2:]], axis=1)
    scores = (
        jnp.einsum(
            "nqhgd,nshd->hgnqs", local_queries, band[:, :, 0], preferred_element_type=jnp.float32
        )
        * score_scale
    )
    relative = jnp.arange(3 * WINDOW)[None, :] - WINDOW - jnp.arange(WINDOW)[:, None]
    key_pos = (
        offset + jnp.arange(blocks)[:, None] * WINDOW - WINDOW + jnp.arange(3 * WINDOW)[None, :]
    )
    valid = (jnp.abs(relative) <= WINDOW)[None] & ((key_pos >= 0) & (key_pos < total_rows))[
        :, None, :
    ]
    scores = jnp.where(valid, scores, -jnp.inf)
    sink = sink_logit.reshape(local_groups, local_size, 1, 1, 1)
    top = jnp.maximum(jnp.max(scores, axis=-1, keepdims=True), sink)
    lifted = jnp.exp(scores - top)
    weights = (lifted / (jnp.sum(lifted, axis=-1, keepdims=True) + jnp.exp(sink - top))).astype(
        jnp.bfloat16
    )
    local_result = jnp.einsum(
        "hgnqs,nshd->nqhgd", weights, band[:, :, 1], preferred_element_type=jnp.float32
    )
    local_result = local_result.astype(jnp.bfloat16).reshape(row_count, local_heads * HEAD)
    joined = lax.psum_scatter(
        jnp.concatenate(
            [
                jnp.dot(grid_result, grid_out_weight, preferred_element_type=jnp.float32),
                jnp.dot(local_result, local_out_weight, preferred_element_type=jnp.float32),
            ],
            axis=1,
        ).astype(jnp.bfloat16),
        "tp",
        scatter_dimension=0,
        tiled=True,
    ).astype(jnp.float32)
    merged = joined[:, :width] + joined[:, width:]
    return merged.astype(jnp.bfloat16)


def solution(mesh):
    in_specs = (
        P("sp", None),
        P(),
        P(None, "tp"),
        P(None, "tp"),
        P(None, "tp"),
        P(),
        P(),
        P(None, "tp"),
        P(None, "tp"),
        P(None, "tp"),
        P("tp"),
        P("tp", None),
        P("tp", None),
    )
    out_specs = P(("sp", "tp"), None)
    return jax.shard_map(shards, mesh=mesh, in_specs=in_specs, out_specs=out_specs, check_vma=False)
```

profile of v0, /device:TPU:0, one launch (start us, length us, event | category | flops | bytes accessed | tf_op | source)
XLA Modules:
  0.0 194.1 jit_solution(18339366877715833661)
XLA Ops:
  6.5 2.7 %fusion.22 = f32[768]{0:T(1024)S(1)} fusion(bf16[768,2048]{1,0:T(8,128)(2,1)} %param.15), kind=kLoop, calls=%fused_computation.27 | loop fusion | flops 4717824 | bytes 3148800 | tf_op jit(solution)/shard_map/reduce_sum | solution.py:32
  10.5 1.0 convolution_convert_fusion.5
  13.6 5.6 %collective-permute-start = (bf16[128,2,1,128]{3,0,2,1:T(8,128)(2,1)}, bf16[128,2,1,128]{3,0,2,1:T(8,128)(2,1)}, u32[]{:S(2)}, u32[]{:S(2)}) collective-permute-start(bf16[128,2,1,128]{3,0,2,1:T(8,128)(2,1)} %get-tuple-element.202), channel_id=1, source_target_pairs={{0,8},{8,16},{16,24},{1,9},{9,17},{17,25},{2,10},{10,18},{18,26},{... | collective-permute-start | bytes 196616 | tf_op jit(solution)/shard_map/ppermute | solution.py:22
  19.2 1.3 collective-permute-start.1
  20.6 1.4 multiply_sine_fusion.1
  23.5 4.0 %convolution_convert_fusion.3 = bf16[768,256]{1,0:T(8,128)(2,1)} fusion(bf16[768,2048]{1,0:T(8,128)(2,1)} %copy-done.4, bf16[2048,256]{1,0:T(8,128)(2,1)} %param.22), kind=kOutput, calls=%fused_computation.39 | convolution fusion | flops 805502976 | bytes 4587520 | tf_op jit(solution)/shard_map/dot_general | solution.py:81
  27.5 3.1 %multiply_reduce_fusion.1 = (f32[768]{0:T(1024)S(1)}, f32[768,128]{0,1:T(8,128)S(1)}) fusion(bf16[768,2048]{1,0:T(8,128)(2,1)} %copy-done.4, bf16[2048,128]{1,0:T(8,128)(2,1)S(1)} %copy-done.21), kind=kOutput, calls=%fused_computation.80 | convolution fusion | flops 403045632 | bytes 4066304 | tf_op jit(solution)/shard_map/dot_general | solution.py:81
  31.6 21.4 %all_gather.6 = bf16[3072,1,128]{0,2,1:T(8,128)(2,1)} all-gather(bf16[768,1,128]{0,2,1:T(8,128)(2,1)S(1)} %pad_maximum_fusion.9), channel_id=1, replica_groups=mesh['sp'=4,'tp'=8] {'sp'}, dimensions={0}, use_global_device_ids=true | all-gather | bytes 983040 | tf_op jit(solution)/shard_map/all_gather | solution.py:126
  53.0 1.1 multiply_reduce_fusion
  54.6 2.3 %slice_negate_fusion.1 = (f32[768,2,32]{2,0,1:T(8,128)}, f32[768,2,32]{2,0,1:T(8,128)}, f32[768,2,32]{2,0,1:T(8,128)}, f32[768,2,32]{2,0,1:T(8,128)}) fusion(f32[768,2,128]{2,0,1:T(8,128)S(1)} %multiply_multiply_fusion), kind=kLoop, calls=%fused_computation.56 | loop fusion | flops 98304 | bytes 1572864 | tf_op jit(solution)/shard_map/neg | solution.py:41
  60.6 3.1 %convolution_convert_fusion.7 = bf16[768,128]{1,0:T(8,128)(2,1)S(1)} fusion(bf16[768,2048]{1,0:T(8,128)(2,1)} %copy-done.4, bf16[2048,128]{1,0:T(8,128)(2,1)} %param.19), kind=kOutput, calls=%fused_computation.47 | convolution fusion | flops 402751488 | bytes 3866624 | tf_op jit(solution)/shard_map/dot_general | solution.py:81
  63.8 17.5 %all-gather = bf16[3072,128]{1,0:T(8,128)(2,1)S(1)} all-gather(bf16[768,128]{1,0:T(8,128)(2,1)S(1)} %convolution_convert_fusion.7), channel_id=2, replica_groups=mesh['sp'=4,'tp'=8] {'sp'}, dimensions={0}, use_global_device_ids=true | all-gather | bytes 983040 | tf_op jit(solution)/shard_map/all_gather | solution.py:127
  82.3 29.1 %while.18 = (s32[]{:T(128)}, f32[1,2,768]{2,1,0:T(2,128)S(1)}, f32[1,2,768]{2,1,0:T(2,128)S(1)}, f32[1,2,768,128]{3,2,1,0:T(8,128)S(1)}, bf16[3072,1,128]{0,2,1:...) while((s32[]{:T(128)}, f32[1,2,768]{2,1,0:T(2,128)S(1)}, ...), condition=%wide.region_6.7_spmd.clone, body=%wide.region_3.6_spmd.clone.sunk | while | flops 1227432960 | bytes 68911312 | solution.py:138
  82.3 6.1 %bitcast_reduce_fusion.2 = (f32[2,768]{1,0:T(2,128)S(1)}, f32[1536,768,2]{1,0,2:T(8,128)}) fusion(bf16[768,1,2,128]{3,0,2,1:T(8,128)(2,1)S(1)} %get-tuple-element.300, bf16[3072,1,128]{0,2,1:T(8,128)(2,1)} %get-tuple-element.299, s32[]{:T(128)S(6)} %select_n.56), kind=kOutput, calls=%fused_computation.1.clone.1 | convolution fusion | flops 608696832 | bytes 10229764 | tf_op jit(solution)/shard_map/while/body/eval_jaxpr/qhgd,shd->hgqs/dot_general | solution.py:105
  88.4 5.4 %fusion.83 = f32[2,768]{1,0:T(2,128)S(1)} fusion(f32[1536,768,2]{1,0,2:T(8,128)} %get-tuple-element.271, f32[2,768]{1,0:T(2,128)S(1)} %bitcast.169), kind=kLoop, calls=%fused_computation.4.clone.1 | loop fusion | flops 7076352 | bytes 9449472 | tf_op jit(solution)/shard_map/while/body/eval_jaxpr/reduce_sum | solution.py:111
  94.8 2.1 %fusion.84 = f32[1,2,768,128]{3,2,1,0:T(8,128)S(1)} fusion(f32[1536,768,2]{1,0,2:T(8,128)S(1)} %copy-done.1, f32[2,768]{1,0:T(2,128)S(1)} %bitcast.170, f32[1,2,768,128]{3,2,1,0:T(8,128)S(1)} %get-tuple-element.287, bf16[3072,1,128]{2,0,1:T(8,128)(2,1)S(1)} %get-tuple-element.301, s32[]{:T(128)S(6)} %select_n.56, ...), kind=kOutput, calls=%fused_computation.8.clone.1 | convolution fusion | flops 611647488 | bytes 11415557 | tf_op jit(solution)/shard_map/while/body/eval_jaxpr/hgqs,shd->hgqd/dot_general | solution.py:112
  96.9 6.1 %bitcast_reduce_fusion.2 = (f32[2,768]{1,0:T(2,128)S(1)}, f32[1536,768,2]{1,0,2:T(8,128)}) fusion(bf16[768,1,2,128]{3,0,2,1:T(8,128)(2,1)S(1)} %get-tuple-element.300, bf16[3072,1,128]{0,2,1:T(8,128)(2,1)} %get-tuple-element.299, s32[]{:T(128)S(6)} %select_n.56), kind=kOutput, calls=%fused_computation.1.clone.1 | convolution fusion | flops 608696832 | bytes 10229764 | tf_op jit(solution)/shard_map/while/body/eval_jaxpr/qhgd,shd->hgqs/dot_general | solution.py:105
  103.0 5.4 %fusion.83 = f32[2,768]{1,0:T(2,128)S(1)} fusion(f32[1536,768,2]{1,0,2:T(8,128)} %get-tuple-element.271, f32[2,768]{1,0:T(2,128)S(1)} %bitcast.169), kind=kLoop, calls=%fused_computation.4.clone.1 | loop fusion | flops 7076352 | bytes 9449472 | tf_op jit(solution)/shard_map/while/body/eval_jaxpr/reduce_sum | solution.py:111
  109.3 2.1 %fusion.84 = f32[1,2,768,128]{3,2,1,0:T(8,128)S(1)} fusion(f32[1536,768,2]{1,0,2:T(8,128)S(1)} %copy-done.1, f32[2,768]{1,0:T(2,128)S(1)} %bitcast.170, f32[1,2,768,128]{3,2,1,0:T(8,128)S(1)} %get-tuple-element.287, bf16[3072,1,128]{2,0,1:T(8,128)(2,1)S(1)} %get-tuple-element.301, s32[]{:T(128)S(6)} %select_n.56, ...), kind=kOutput, calls=%fused_computation.8.clone.1 | convolution fusion | flops 611647488 | bytes 11415557 | tf_op jit(solution)/shard_map/while/body/eval_jaxpr/hgqs,shd->hgqd/dot_general | solution.py:112
  111.8 2.7 %convolution_convert_fusion.1 = bf16[768,2048]{1,0:T(8,128)(2,1)} fusion(bf16[768,256]{0,1:T(8,128)(2,1)S(1)} %bitcast.172, bf16[256,2048]{1,0:T(8,128)(2,1)S(1)} %copy-done), kind=kOutput, calls=%fused_computation.32 | convolution fusion | flops 806879232 | bytes 4587520 | tf_op jit(solution)/shard_map/dot_general | solution.py:186
  118.8 1.0 convolution_convert_fusion
  120.7 3.4 %pad_maximum_fusion = bf16[768,4096]{1,0:T(8,128)(2,1)} fusion(bf16[768,2048]{1,0:T(8,128)(2,1)S(1)} %convolution_convert_fusion, bf16[768,2048]{1,0:T(8,128)(2,1)S(1)} %copy-done.2), kind=kLoop, calls=%fused_computation.30 | loop fusion | flops 12582912 | bytes 12582912 | tf_op jit(solution)/shard_map/concatenate | solution.py:184
  124.1 61.0 %reduce-scatter.2.cloned.1.call-done = bf16[96,4096]{1,0:T(8,128)(2,1)} async-done(((bf16[768,4096]{1,0:T(8,128)(2,1)}), bf16[96,4096]{1,0:T(8,128)(2,1)}) %reduce-scatter.2.cloned.1.call-update) | async-done | bytes 786448 | tf_op jit(solution)/shard_map/reduce_scatter | solution.py:183
  185.1 1.3 convert_element_type.122
  (119 shorter events, 19.2 us)
Async XLA Ops:
  6.5 105.2 %copy-start = (bf16[256,2048]{1,0:T(8,128)(2,1)S(1)}, bf16[256,2048]{1,0:T(8,128)(2,1)}, u32[]{:S(2)}) copy-start(bf16[256,2048]{1,0:T(8,128)(2,1)} %param.26) | copy-start | bytes 3145732
  6.5 178.6 %reduce-scatter.2.cloned.1.call-start = ((), (), s32[]{:S(2)}) async-start(), calls=%async_computation.1 | async-start | bytes 7077888 | tf_op jit(solution)/shard_map/reduce_scatter | solution.py:183
  6.5 2.9 %copy-start.3 = (bf16[768,2048]{1,0:T(8,128)(2,1)S(1)}, bf16[768,2048]{1,0:T(8,128)(2,1)}, u32[]{:S(2)}) copy-start(bf16[768,2048]{1,0:T(8,128)(2,1)} %param.15) | copy-start | bytes 9437188
  13.6 101.5 %collective-permute-start = (bf16[128,2,1,128]{3,0,2,1:T(8,128)(2,1)}, bf16[128,2,1,128]{3,0,2,1:T(8,128)(2,1)}, u32[]{:S(2)}, u32[]{:S(2)}) collective-permute-start(bf16[128,2,1,128]{3,0,2,1:T(8,128)(2,1)} %get-tuple-element.202), channel_id=1, source_target_pairs={{0,8},{8,16},{16,24},{1,9},{9,17},{17,25},{2,10},{10,18},{18,26},{... | collective-permute-start | bytes 196616 | tf_op jit(solution)/shard_map/ppermute | solution.py:22
  19.2 95.9 %collective-permute-start.1 = (bf16[128,2,1,128]{3,0,2,1:T(8,128)(2,1)}, bf16[128,2,1,128]{3,0,2,1:T(8,128)(2,1)}, u32[]{:S(2)}, u32[]{:S(2)}) collective-permute-start(bf16[128,2,1,128]{3,0,2,1:T(8,128)(2,1)} %get-tuple-element.203), channel_id=1, source_target_pairs={{8,0},{16,8},{24,16},{9,1},{17,9},{25,17},{10,2},{18,10},{26,18},{... | collective-permute-start | bytes 196616 | tf_op jit(solution)/shard_map/ppermute | solution.py:25
  23.5 4.0 %copy-start.21 = (bf16[2048,128]{1,0:T(8,128)(2,1)S(1)}, bf16[2048,128]{1,0:T(8,128)(2,1)}, u32[]{:S(2)}) copy-start(bf16[2048,128]{1,0:T(8,128)(2,1)} %param.18) | copy-start | bytes 1572868
  27.5 3.1 %copy-start.28 = (f32[128]{0:T(128)S(1)}, f32[128]{0:T(128)}, u32[]{:S(2)}) copy-start(f32[128]{0:T(128)} %param.21) | copy-start | bytes 1540
  30.6 22.4 %copy-start.5 = (bf16[768,2048]{1,0:T(8,128)(2,1)S(1)}, bf16[768,2048]{1,0:T(8,128)(2,1)}, u32[]{:S(2)}) copy-start(bf16[768,2048]{1,0:T(8,128)(2,1)} %copy-done.4) | copy-start | bytes 9437188
  30.6 22.4 %copy-start.29 = (bf16[2048,256]{1,0:T(8,128)(2,1)S(1)}, bf16[2048,256]{1,0:T(8,128)(2,1)}, u32[]{:S(2)}) copy-start(bf16[2048,256]{1,0:T(8,128)(2,1)} %param.17) | copy-start | bytes 3145732
  54.5 3.3 %copy-start.20 = (f32[768,64]{0,1:T(8,128)S(1)}, f32[768,64]{0,1:T(8,128)}, u32[]{:S(2)}) copy-start(f32[768,64]{0,1:T(8,128)} %get-tuple-element.205) | copy-start | bytes 589828
  54.6 5.1 %copy-start.19 = (f32[768,64]{0,1:T(8,128)S(1)}, f32[768,64]{0,1:T(8,128)}, u32[]{:S(2)}) copy-start(f32[768,64]{0,1:T(8,128)} %get-tuple-element.204) | copy-start | bytes 589828
  60.6 20.7 %copy-start.6 = (f32[768,2,32]{2,0,1:T(8,128)S(1)}, f32[768,2,32]{2,0,1:T(8,128)}, u32[]{:S(2)}) copy-start(f32[768,2,32]{2,0,1:T(8,128)} %get-tuple-element.190) | copy-start | bytes 589828
  60.6 20.7 %copy-start.7 = (f32[768,2,32]{2,0,1:T(8,128)S(1)}, f32[768,2,32]{2,0,1:T(8,128)}, u32[]{:S(2)}) copy-start(f32[768,2,32]{2,0,1:T(8,128)} %get-tuple-element.191) | copy-start | bytes 589828
  60.6 20.7 %copy-start.8 = (f32[768,2,32]{2,0,1:T(8,128)S(1)}, f32[768,2,32]{2,0,1:T(8,128)}, u32[]{:S(2)}) copy-start(f32[768,2,32]{2,0,1:T(8,128)} %get-tuple-element.192) | copy-start | bytes 589828
  60.6 20.7 %copy-start.9 = (f32[768,2,32]{2,0,1:T(8,128)S(1)}, f32[768,2,32]{2,0,1:T(8,128)}, u32[]{:S(2)}) copy-start(f32[768,2,32]{2,0,1:T(8,128)} %get-tuple-element.193) | copy-start | bytes 589828
  60.6 20.7 %copy-start.14 = (f32[768,64]{1,0:T(8,128)S(1)}, f32[768,64]{1,0:T(8,128)}, u32[]{:S(2)}) copy-start(f32[768,64]{1,0:T(8,128)} %copy.29) | copy-start | bytes 589828
  60.6 20.7 %copy-start.15 = (f32[768,64]{1,0:T(8,128)S(1)}, f32[768,64]{1,0:T(8,128)}, u32[]{:S(2)}) copy-start(f32[768,64]{1,0:T(8,128)} %copy.28) | copy-start | bytes 589828
  60.6 20.7 %copy-start.16 = (f32[768,64]{1,0:T(8,128)S(1)}, f32[768,64]{1,0:T(8,128)}, u32[]{:S(2)}) copy-start(f32[768,64]{1,0:T(8,128)} %copy.31) | copy-start | bytes 589828
  60.6 20.7 %copy-start.17 = (f32[768,64]{1,0:T(8,128)S(1)}, f32[768,64]{1,0:T(8,128)}, u32[]{:S(2)}) copy-start(f32[768,64]{1,0:T(8,128)} %copy.30) | copy-start | bytes 589828
  88.4 6.4 %copy-start.1 = (f32[1536,768,2]{1,0,2:T(8,128)S(1)}, f32[1536,768,2]{1,0,2:T(8,128)}, u32[]{:S(2)}) copy-start(f32[1536,768,2]{1,0,2:T(8,128)} %get-tuple-element.271) | copy-start | bytes 28311556 | tf_op jit(solution)/shard_map/while
  103.0 6.4 %copy-start.1 = (f32[1536,768,2]{1,0,2:T(8,128)S(1)}, f32[1536,768,2]{1,0,2:T(8,128)}, u32[]{:S(2)}) copy-start(f32[1536,768,2]{1,0,2:T(8,128)} %get-tuple-element.271) | copy-start | bytes 28311556 | tf_op jit(solution)/shard_map/while
  111.8 3.2 %copy-start.22 = (bf16[768,256]{1,0:T(8,128)(2,1)S(1)}, bf16[768,256]{1,0:T(8,128)(2,1)}, u32[]{:S(2)}) copy-start(bf16[768,256]{1,0:T(8,128)(2,1)} %convolution_convert_fusion.3) | copy-start | bytes 1179652
  111.8 3.3 %copy-start.11 = (bf16[768,128]{1,0:T(8,128)(2,1)S(1)}, bf16[768,128]{1,0:T(8,128)(2,1)}, u32[]{:S(2)}) copy-start(bf16[768,128]{1,0:T(8,128)(2,1)} %copy-done.10) | copy-start | bytes 589828
  111.8 3.3 %copy-start.13 = (bf16[768,128]{1,0:T(8,128)(2,1)S(1)}, bf16[768,128]{1,0:T(8,128)(2,1)}, u32[]{:S(2)}) copy-start(bf16[768,128]{1,0:T(8,128)(2,1)} %copy-done.12) | copy-start | bytes 589828
  (12 other events, 19.5 us)
Sparse Core Ops, SparseCore 0:
  124.2 60.8 reduce-scatter.1
where the time goes:
time: 195 us; the launch traced here: 194 us
  waiting for transfers between devices  61 us (31%)
  blocking collectives  38.9 us (20%)
  matrix products  34.5 us (18%)
  other arithmetic  30.3 us (16%)
  between operations  13.9 us (7%)
  local copies, waits for them, and re-layouts  8.42 us (4%)
  starting transfers between devices  6.86 us (4%)
    reduce_scatter x1, waiting for transfers between devices, shards(): lax.psum_scatter(jnp.concatenate([jnp.dot(grid_result, grid_out_weight, p...  61 us
    all_gather x1, blocking collectives, shards(): lax.all_gather(keys, 'sp', axis=0, tiled=True)  21.4 us
    all_gather x1, blocking collectives, shards(): lax.all_gather(values, 'sp', axis=0, tiled=True)  17.5 us
    dot_general x6, matrix products, project(): jnp.dot(normed, weight, preferred_element_type=jnp.float32)  13.2 us
    dot_general x2, matrix products, absorb(): jnp.einsum('qhgd,shd->hgqs', queries, pieces[0], preferred_element_type=j...  12.2 us
    reduce_sum x2, other arithmetic, absorb(): totals = totals * factor + jnp.sum(weights, axis=-1)  10.7 us
    ppermute x1, starting transfers between devices, padded(): lax.ppermute(lax.slice_in_dim(block, block.shape[dim] - width, None, axis...  5.58 us
    dot_general x2, matrix products, absorb(): jnp.einsum('hgqs,shd->hgqd', weights.astype(jnp.bfloat16), pieces[1], pre...  4.15 us
  transfers between devices with their start and end apart: 3, of which 1 were waited for; matrix products, arithmetic and copies ran while one was open for 27% of the time, Pallas kernels for 0%

commit v1 on v0

v1 whole, which is shorter than its diff:
```python
import functools

import jax
import jax.numpy as jnp
import numpy as np
from jax import lax
from jax.experimental import pallas as pl
from jax.experimental.pallas import tpu as pltpu
from jax.sharding import PartitionSpec as P

HEAD = 128
WINDOW = 128
GRID_W = 64
EPSILON = 1e-06
ROPE_BASE = 10000.0
PIECE = 32
CHUNK = 256
LOG2E = 1.4426950408889634
SCALE = HEAD ** (-0.5)
MESH = pl.DeviceIdType.MESH


def rotary_tables(total_rows):
    half = HEAD // 2
    inverse = (ROPE_BASE ** (-np.arange(0, half, 2, dtype=np.float32) / half)).astype(np.float32)

    def table(count, low):
        angle = np.arange(count, dtype=np.float32)[:, None] * inverse
        cosine = np.cos(angle).astype(np.float32)
        sine = np.sin(angle).astype(np.float32)
        zero = np.zeros((count, half), np.float32)
        cosine = np.concatenate([cosine, cosine], axis=1)
        sine = np.concatenate([-sine, sine], axis=1)
        order = (lambda x: [x, zero]) if low else (lambda x: [zero, x])
        return np.stack(
            [np.concatenate(order(cosine), axis=1), np.concatenate(order(sine), axis=1)]
        )

    return table(total_rows // GRID_W, True), table(GRID_W, False)


def dot(a, b):
    return jnp.dot(a, b, preferred_element_type=jnp.float32)


def dot_t(a, b):
    return lax.dot_general(a, b, (((1,), (1,)), ((), ())), preferred_element_type=jnp.float32)


def with_ones(v):
    return jnp.concatenate([v, jnp.ones((v.shape[0], HEAD), v.dtype)], axis=1)


def kernel(
    n_sp, n_tp, rows, width,
    tokens, gain, gqw, gkw, gvw, gq_gain, gk_gain, lqw, lkw, lvw, sink, gow, low, row_tab, col_tab,
    out,
    tok_v, normed, wkv, wq, wo, kv, lkv, q_s, lq_s, lo_s, acc, m_s, pbuf, rbuf0, sbuf, rbuf1,
    in_sem, kv_recv, kv_send, fwd_send, halo_recv, halo_send, r0_send, r0_recv, r1_send, r1_recv,
):
    me = lax.axis_index("sp")
    tp = lax.axis_index("tp")
    par = lax.rem(tp, 2)
    chip = tp // 2
    chips = n_tp // 2
    units = rows // (n_tp * PIECE)
    unit_rows = n_tp * PIECE
    partner = tp + 1 - 2 * par

    chunks = rows // CHUNK
    loads = []

    def load(src, dst):
        copy = pltpu.make_async_copy(src, dst, in_sem.at[len(loads)])
        copy.start()
        loads.append(copy)

    load(tokens.at[pl.ds(0, CHUNK)], tok_v.at[pl.ds(0, CHUNK)])
    for i, w in enumerate((gkw, gvw, lkw, lvw)):
        load(w, wkv.at[:, pl.ds(i * HEAD, HEAD)])
    load(tokens.at[pl.ds(CHUNK, rows - CHUNK)], tok_v.at[pl.ds(CHUNK, rows - CHUNK)])
    load(gqw, wq.at[:, pl.ds(0, 2 * HEAD)])
    load(lqw, wq.at[:, pl.ds(2 * HEAD, 2 * HEAD)])
    load(gow, wo.at[pl.ds(0, 2 * HEAD)])
    load(low, wo.at[pl.ds(2 * HEAD, 2 * HEAD)])

    barrier = pltpu.get_barrier_semaphore()
    for step in (-2, -1, 1, 2):
        other = me + step

        @pl.when((other >= 0) & (other < n_sp))
        def _():
            pl.semaphore_signal(barrier, inc=1, device_id={"sp": other}, device_id_type=MESH)

    pl.semaphore_signal(barrier, inc=1, device_id={"tp": partner}, device_id_type=MESH)
    for k in range(1, chips):
        peer = lax.rem(chip + k, chips) * 2 + par
        pl.semaphore_signal(barrier, inc=1, device_id={"tp": peer}, device_id_type=MESH)
    near = jnp.minimum(me, 2) + jnp.minimum(n_sp - 1 - me, 2)
    pl.semaphore_wait(barrier, near + chips)

    def norm_heads(x, head_gain):
        return x * lax.rsqrt(jnp.mean(x * x, axis=-1, keepdims=True) + EPSILON) * head_gain

    def rotary(x, group, count):
        def tiled(k):
            return jnp.concatenate(
                [row_tab[k, pl.ds(group + i, 1), :] + col_tab[k] for i in range(count // GRID_W)],
                axis=0,
            )

        lane = lax.broadcasted_iota(jnp.int32, x.shape, 1)
        quarter = HEAD // 4
        first = lax.rem(lane, 2 * quarter) < quarter
        turned = jnp.where(
            first, pltpu.roll(x, HEAD - quarter, 1), pltpu.roll(x, quarter, 1)
        )
        return x * tiled(0) + turned * tiled(1)

    def place(g):
        t = g // units
        return lax.rem(g, units), lax.rem(t, 2) * chips + t // 2

    first_group = me * (rows // GRID_W)

    loads[0].wait()
    for i in range(1, 5):
        loads[i].wait()

    def kv_chunk(c):
        at = pl.multiple_of(c * CHUNK, CHUNK)
        wide = tok_v[pl.ds(at, CHUNK), :].astype(jnp.float32)
        mean = jnp.mean(wide * wide, axis=-1, keepdims=True)
        scaled = (wide * lax.rsqrt(mean + EPSILON) * gain[...]).astype(jnp.bfloat16)
        normed[pl.ds(at, CHUNK), :] = scaled
        made = dot(scaled, wkv[...]).astype(jnp.bfloat16)
        key = norm_heads(made[:, :HEAD].astype(jnp.float32), gk_gain[...])
        key = rotary(key, first_group + c * (CHUNK // GRID_W), CHUNK)
        kv[me, pl.ds(at, CHUNK), 0:HEAD] = key.astype(jnp.bfloat16)
        kv[me, pl.ds(at, CHUNK), HEAD:] = made[:, HEAD : 2 * HEAD]
        lkv[pl.ds(pl.multiple_of(WINDOW + at, WINDOW), CHUNK), :] = made[:, 2 * HEAD :]

    kv_chunk(0)
    loads[5].wait()

    @pl.loop(1, chunks)
    def _(c):
        kv_chunk(c)

    def halo_copy(right):
        src, dst = (rows, 0) if right else (WINDOW, WINDOW + rows)
        return pltpu.make_async_remote_copy(
            src_ref=lkv.at[pl.ds(src, WINDOW)],
            dst_ref=lkv.at[pl.ds(dst, WINDOW)],
            send_sem=halo_send.at[int(right)],
            recv_sem=halo_recv.at[int(right)],
            device_id={"sp": me + (1 if right else -1)},
            device_id_type=MESH,
        )

    def kv_copy(slot, to, sem):
        return pltpu.make_async_remote_copy(
            src_ref=kv.at[slot],
            dst_ref=kv.at[slot],
            send_sem=sem,
            recv_sem=kv_recv.at[slot],
            device_id={"sp": to},
            device_id_type=MESH,
        )

    has_right = me < n_sp - 1
    has_left = me > 0

    @pl.when(has_right)
    def _():
        halo_copy(True).start()

    @pl.when(has_left)
    def _():
        halo_copy(False).start()

    @pl.when(jnp.logical_not(has_left))
    def _():
        lkv[pl.ds(0, WINDOW), :] = jnp.zeros((WINDOW, 2 * HEAD), jnp.bfloat16)

    @pl.when(jnp.logical_not(has_right))
    def _():
        lkv[pl.ds(WINDOW + rows, WINDOW), :] = jnp.zeros((WINDOW, 2 * HEAD), jnp.bfloat16)

    own_sends = ((1, 0), (-1, 1), (2, 2), (-2, 3))
    for step, index in own_sends:
        other = me + step

        @pl.when((other >= 0) & (other < n_sp))
        def _():
            kv_copy(me, other, kv_send.at[index]).start()

    loads[6].wait()
    loads[7].wait()

    @pl.loop(0, chunks)
    def _(c):
        at = pl.multiple_of(c * CHUNK, CHUNK)
        made = dot(normed[pl.ds(at, CHUNK), :], wq[...]).astype(jnp.bfloat16)
        lq_s[pl.ds(at, CHUNK), :] = made[:, 2 * HEAD :]
        for h in range(2):
            x = norm_heads(made[:, h * HEAD : (h + 1) * HEAD].astype(jnp.float32), gq_gain[...])
            x = rotary(x, first_group + c * (CHUNK // GRID_W), CHUNK).astype(jnp.bfloat16)
            for i in range(CHUNK // PIECE):
                u, pos = place(c * (CHUNK // PIECE) + i)
                q_s[u, h, pos] = x[i * PIECE : (i + 1) * PIECE]

    def attend(u, slot, start):
        k = kv[slot, :, 0:HEAD]
        v = with_ones(kv[slot, :, HEAD:])
        for h in range(2):
            q = q_s[u, h].reshape(unit_rows, HEAD)
            s = dot_t(q, k)
            top = jnp.max(s, axis=-1, keepdims=True)
            if start:
                new = top
            else:
                old = m_s[u, h][:, 0:1]
                new = jnp.maximum(old, top)
            p = jnp.exp2((s - new) * (SCALE * LOG2E)).astype(jnp.bfloat16)
            part = dot(p, v)
            if start:
                acc[u, h] = part
            else:
                acc[u, h] = acc[u, h] * jnp.exp2((old - new) * (SCALE * LOG2E)) + part
            m_s[u, h] = jnp.broadcast_to(new, (unit_rows, HEAD))

    @pl.loop(0, units)
    def _(u):
        attend(u, me, True)

    @pl.when(has_left)
    def _():
        halo_copy(True).wait_recv()

    @pl.when(has_right)
    def _():
        halo_copy(False).wait_recv()

    shape = (2 * WINDOW, 3 * WINDOW)
    query_row = lax.broadcasted_iota(jnp.int32, shape, 0)
    query_row = jnp.where(query_row >= WINDOW, query_row - WINDOW, query_row)
    key_col = lax.broadcasted_iota(jnp.int32, shape, 1)
    relative = key_col - WINDOW - query_row
    in_band = (relative <= WINDOW) & (relative >= -WINDOW)
    second = lax.broadcasted_iota(jnp.int32, (2 * WINDOW, 1), 0) >= WINDOW

    @pl.loop(0, rows // WINDOW)
    def _(n):
        at = pl.multiple_of(n * WINDOW, WINDOW)
        q = jnp.concatenate(
            [lq_s[pl.ds(at, WINDOW), 0:HEAD], lq_s[pl.ds(at, WINDOW), HEAD:]], axis=0
        )
        s = dot_t(q, lkv[pl.ds(at, 3 * WINDOW), 0:HEAD]) * SCALE
        key_pos = me * rows + n * WINDOW - WINDOW + key_col
        valid = in_band & (key_pos >= 0) & (key_pos < n_sp * rows)
        s = jnp.where(valid, s, -jnp.inf)
        drain = jnp.where(second, sink[1], sink[0])
        top = jnp.maximum(jnp.max(s, axis=-1, keepdims=True), drain)
        p = jnp.exp(s - top).astype(jnp.bfloat16)
        r = dot(p, with_ones(lkv[pl.ds(at, 3 * WINDOW), HEAD:]))
        r = (r[:, :HEAD] / (r[:, HEAD:] + jnp.exp(drain - top))).astype(jnp.bfloat16)
        for i in range(WINDOW // PIECE):
            u, pos = place(n * (WINDOW // PIECE) + i)
            for h in range(2):
                lo_s[u, pos, :, h * HEAD : (h + 1) * HEAD] = r[
                    h * WINDOW + i * PIECE : h * WINDOW + (i + 1) * PIECE
                ]

    both = jnp.minimum(me, n_sp - 1 - me)
    lean = jnp.where(me < n_sp - 1 - me, 1, -1)

    def block_of(j):
        odd = lax.rem(j, 2)
        paired = me + ((j + 1) // 2) * (2 * odd - 1)
        alone = me + lean * (j - both)
        return jnp.where(j <= 2 * both, paired, alone)

    def onward(slot):
        away = slot - me
        to = jnp.where(away > 0, me - 1, me + 1)
        far = (away >= 2) | (away <= -2)
        return to, far & (to >= 0) & (to < n_sp)

    def arrive(j):
        slot = block_of(j)
        kv_copy(slot, jnp.where(has_left, me - 1, me + 1), fwd_send.at[slot]).wait_recv()
        to, goes = onward(slot)

        @pl.when(goes)
        def _():
            kv_copy(slot, to, fwd_send.at[slot]).start()

        return slot

    @pl.loop(1, n_sp - 1)
    def _(j):
        slot = arrive(j)

        @pl.loop(0, units)
        def _(u):
            attend(u, slot, False)

    def pair_copy(u):
        return pltpu.make_async_remote_copy(
            src_ref=pbuf.at[u, pl.ds((1 - par) * chips, chips)],
            dst_ref=rbuf0.at[u],
            send_sem=r0_send.at[u],
            recv_sem=r0_recv.at[u],
            device_id={"tp": partner},
            device_id_type=MESH,
        )

    def chip_copy(u, k):
        to = lax.rem(chip + k, chips)
        return pltpu.make_async_remote_copy(
            src_ref=sbuf.at[u, k - 1],
            dst_ref=rbuf1.at[u, k - 1],
            send_sem=r1_send.at[u, k - 1],
            recv_sem=r1_recv.at[u, k - 1],
            device_id={"tp": to * 2 + par},
            device_id_type=MESH,
        )

    def spread(u):
        pair_copy(u).wait_recv()
        for k in range(1, chips):
            to = lax.rem(chip + k, chips)
            total = pbuf[u, par * chips + to].astype(jnp.float32) + rbuf0[u, to].astype(
                jnp.float32
            )
            sbuf[u, k - 1] = total.astype(jnp.bfloat16)
            chip_copy(u, k).start()

    last = arrive(n_sp - 1)
    loads[8].wait()
    loads[9].wait()
    tile = 512

    @pl.loop(0, units)
    def _(u):
        attend(u, last, False)
        heads = [(acc[u, h][:, :HEAD] / acc[u, h][:, HEAD:]).astype(jnp.bfloat16) for h in range(2)]
        mixed = jnp.concatenate(heads + [lo_s[u].reshape(unit_rows, 2 * HEAD)], axis=1)
        for i in range(width // tile):
            part = dot(mixed, wo[:, i * tile : (i + 1) * tile]).astype(jnp.bfloat16)
            pbuf[u, :, :, i * tile : (i + 1) * tile] = part.reshape(n_tp, PIECE, tile)
        pair_copy(u).start()

        @pl.when(u > 0)
        def _():
            spread(u - 1)

    spread(units - 1)

    @pl.loop(0, units)
    def _(u):
        total = pbuf[u, par * chips + chip].astype(jnp.float32) + rbuf0[u, chip].astype(
            jnp.float32
        )
        for k in range(1, chips):
            chip_copy(u, k).wait_recv()
            total = total + rbuf1[u, k - 1].astype(jnp.float32)
        out[pl.ds(pl.multiple_of(u * PIECE, PIECE), PIECE), :] = total.astype(jnp.bfloat16)

    @pl.loop(0, units)
    def _(u):
        pair_copy(u).wait_send()
        for k in range(1, chips):
            chip_copy(u, k).wait_send()

    @pl.when(has_right)
    def _():
        halo_copy(True).wait_send()

    @pl.when(has_left)
    def _():
        halo_copy(False).wait_send()

    for step, index in own_sends:
        other = me + step

        @pl.when((other >= 0) & (other < n_sp))
        def _():
            kv_copy(me, other, kv_send.at[index]).wait_send()

    @pl.loop(1, n_sp)
    def _(j):
        slot = block_of(j)
        to, goes = onward(slot)

        @pl.when(goes)
        def _():
            kv_copy(slot, to, fwd_send.at[slot]).wait_send()


def solution(mesh):
    n_sp, n_tp = mesh.shape["sp"], mesh.shape["tp"]

    def shards(
        tokens, norm_gain, gqw, gkw, gvw, gq_gain, gk_gain, lqw, lkw, lvw, sink, gow, low
    ):
        rows, depth = tokens.shape
        width = gow.shape[1]
        units = rows // (n_tp * PIECE)
        unit_rows = n_tp * PIECE
        chips = n_tp // 2
        row_tab, col_tab = rotary_tables(rows * n_sp)
        vmem = pl.BlockSpec(memory_space=pltpu.VMEM)
        hbm = pl.BlockSpec(memory_space=pl.ANY)
        smem = pl.BlockSpec(memory_space=pltpu.SMEM)
        bf16, f32 = jnp.bfloat16, jnp.float32
        dma = pltpu.SemaphoreType.DMA
        return pl.pallas_call(
            functools.partial(kernel, n_sp, n_tp, rows, width),
            out_shape=jax.ShapeDtypeStruct((rows // n_tp, width), bf16),
            in_specs=[
                hbm, vmem, hbm, hbm, hbm, vmem, vmem, hbm, hbm, hbm, smem, hbm, hbm, vmem, vmem
            ],
            out_specs=vmem,
            scratch_shapes=[
                pltpu.VMEM((rows, depth), bf16),
                pltpu.VMEM((rows, depth), bf16),
                pltpu.VMEM((depth, 4 * HEAD), bf16),
                pltpu.VMEM((depth, 4 * HEAD), bf16),
                pltpu.VMEM((4 * HEAD, width), bf16),
                pltpu.VMEM((n_sp, rows, 2 * HEAD), bf16),
                pltpu.VMEM((rows + 2 * WINDOW, 2 * HEAD), bf16),
                pltpu.VMEM((units, 2, n_tp, PIECE, HEAD), bf16),
                pltpu.VMEM((rows, 2 * HEAD), bf16),
                pltpu.VMEM((units, n_tp, PIECE, 2 * HEAD), bf16),
                pltpu.VMEM((units, 2, unit_rows, 2 * HEAD), f32),
                pltpu.VMEM((units, 2, unit_rows, HEAD), f32),
                pltpu.VMEM((units, n_tp, PIECE, width), bf16),
                pltpu.VMEM((units, chips, PIECE, width), bf16),
                pltpu.VMEM((units, chips - 1, PIECE, width), bf16),
                pltpu.VMEM((units, chips - 1, PIECE, width), bf16),
                dma((10,)),
                dma((n_sp,)),
                dma((4,)),
                dma((n_sp,)),
                dma((2,)),
                dma((2,)),
                dma((units,)),
                dma((units,)),
                dma((units, chips - 1)),
                dma((units, chips - 1)),
            ],
            compiler_params=pltpu.CompilerParams(
                collective_id=0, has_side_effects=True, vmem_limit_bytes=60 * 2**20
            ),
            name="attention",
        )(
            tokens, norm_gain.reshape(1, depth), gqw, gkw, gvw,
            gq_gain.reshape(1, HEAD), gk_gain.reshape(1, HEAD), lqw, lkw, lvw,
            sink, gow, low, jnp.asarray(row_tab), jnp.asarray(col_tab),
        )

    in_specs = (
        P("sp", None),
        P(),
        P(None, "tp"),
        P(None, "tp"),
        P(None, "tp"),
        P(),
        P(),
        P(None, "tp"),
        P(None, "tp"),
        P(None, "tp"),
        P("tp"),
        P("tp", None),
        P("tp", None),
    )
    out_specs = P(("sp", "tp"), None)
    return jax.shard_map(shards, mesh=mesh, in_specs=in_specs, out_specs=out_specs, check_vma=False)
```

time: 195 us -> 72.3 us (0.37)
  Pallas kernels: 0 us -> 70.3 us
  waiting for transfers between devices: 61 us -> 0 us
  blocking collectives: 38.9 us -> 0 us
  matrix products: 34.5 us -> 0 us
  other arithmetic: 30.3 us -> 0 us
  between operations: 13.9 us -> 0.01 us
  starting transfers between devices: 6.86 us -> 0 us
  local copies, waits for them, and re-layouts: 8.42 us -> 1.77 us
    pallas_call x0 -> x1, Pallas kernels: none -> 70.3 us  [shards(): pl.pallas_call(functools.partial(kernel, n_sp, n_tp, rows, width), out_sh...]
    reduce_scatter x1 -> x0, waiting for transfers between devices: 61 us -> none  [shards(): lax.psum_scatter(jnp.concatenate([jnp.dot(grid_result, grid_out_weight, p...]
    all_gather x2 -> x0, blocking collectives: 38.9 us -> none  [the longest x1 21.4 us: shards(): lax.all_gather(keys, 'sp', axis=0, tiled=True)]
    dot_general x14 -> x0, matrix products: 34.5 us -> none  [the longest x6 13.2 us: project(): jnp.dot(normed, weight, preferred_element_type=jnp.float32)]
    reduce_sum x4 -> x0, other arithmetic: 14 us -> none  [the longest x2 10.7 us: absorb(): totals = totals * factor + jnp.sum(weights, axis=-1)]
    ppermute x2 -> x0, starting transfers between devices: 6.86 us -> none  [the longest x1 5.58 us: padded(): lax.ppermute(lax.slice_in_dim(block, block.shape[dim] - width, None, axis...]
    concatenate x7 -> x0, other arithmetic: 6.11 us -> none  [the longest x1 3.44 us: shards(): jnp.concatenate([jnp.dot(grid_result, grid_out_weight, preferred_element_...]
    mul x4 -> x0, local copies, waits for them, and re-layouts: 3.67 us -> none  [half_turn(): return part * cosine + turned * sine]
  transfers between devices with their start and end apart: 3 -> 0, of which waited for: 1 -> 0; matrix products, arithmetic and copies ran while one was open for 27% -> 0% of each run, Pallas kernels for 0% -> 0%
where the time goes in v1:
time: 72.3 us; the launch traced here: 72.1 us
  Pallas kernels  70.3 us (97%)
  local copies, waits for them, and re-layouts  1.77 us (2%)
    pallas_call x1, Pallas kernels, shards(): pl.pallas_call(functools.partial(kernel, n_sp, n_tp, rows, width), out_sh...  70.3 us
    unnamed x1, local copies, waits for them, and re-layouts  1.77 us

profile of v1, /device:TPU:0, one launch (start us, length us, event | category | flops | bytes accessed | tf_op | source)
XLA Modules:
  0.0 72.1 jit_solution(14110957165043395638)
XLA Ops:
  0.0 70.3 %attention.1 = bf16[96,2048]{1,0:T(8,128)(2,1)} custom-call(bf16[768,2048]{1,0:T(8,128)(2,1)} %tokens.1, f32[1,2048]{1,0:T(1,128)} %bitcast.3, bf16[2048,256]{1,0:T(8,128)(2,1)} %gqw.1, bf16[2048,128]{1,0:T(8,128)(2,1)} %gkw.1, bf16[2048,128]{1,0:T(8,128)(2,1)} %gvw.1, f32[1,128]{1,0:T(1,128)} %bitcast.4, f32[1,128]{1,0:T(1,128)} %bitcast.5, ...), custom_call_target="tpu_custom_call" | custom-call | tf_op jit(solution)/shard_map/attention/pallas_call | solution.py:419
  70.4 1.8 %copy.17 = bf16[96,2048]{1,0:T(8,128)(2,1)} copy(bf16[96,2048]{1,0:T(8,128)(2,1)} %attention.1) | data formatting | bytes 786432

commit v2 on v1

--- a/solution.py
+++ b/solution.py
@@ -56,7 +56,7 @@
     tokens, gain, gqw, gkw, gvw, gq_gain, gk_gain, lqw, lkw, lvw, sink, gow, low, row_tab, col_tab,
     out,
     tok_v, normed, wkv, wq, wo, kv, lkv, q_s, lq_s, lo_s, acc, m_s, pbuf, rbuf0, sbuf, rbuf1,
-    in_sem, kv_recv, kv_send, fwd_send, halo_recv, halo_send, r0_send, r0_recv, r1_send, r1_recv,
+    in_sem, kv_recv, kv_send, halo_recv, halo_send, r0_send, r0_recv, r1_send, r1_recv,
 ):
     me = lax.axis_index("sp")
     tp = lax.axis_index("tp")
@@ -85,7 +85,7 @@
     load(low, wo.at[pl.ds(2 * HEAD, 2 * HEAD)])
 
     barrier = pltpu.get_barrier_semaphore()
-    for step in (-2, -1, 1, 2):
+    for step in (-1, 1):
         other = me + step
 
         @pl.when((other >= 0) & (other < n_sp))
@@ -96,7 +96,7 @@
     for k in range(1, chips):
         peer = lax.rem(chip + k, chips) * 2 + par
         pl.semaphore_signal(barrier, inc=1, device_id={"tp": peer}, device_id_type=MESH)
-    near = jnp.minimum(me, 2) + jnp.minimum(n_sp - 1 - me, 2)
+    near = jnp.minimum(me, 1) + jnp.minimum(n_sp - 1 - me, 1)
     pl.semaphore_wait(barrier, near + chips)
 
     def norm_heads(x, head_gain):
@@ -122,6 +122,40 @@
         return lax.rem(g, units), lax.rem(t, 2) * chips + t // 2
 
     first_group = me * (rows // GRID_W)
+
+    has_right = me < n_sp - 1
+    has_left = me > 0
+    order = [0] + [chunks - 1] * (chunks > 1) + list(range(1, chunks - 1))
+
+    def halo_copy(right):
+        src, dst = (rows, 0) if right else (WINDOW, WINDOW + rows)
+        return pltpu.make_async_remote_copy(
+            src_ref=lkv.at[pl.ds(src, WINDOW)],
+            dst_ref=lkv.at[pl.ds(dst, WINDOW)],
+            send_sem=halo_send.at[int(right)],
+            recv_sem=halo_recv.at[int(right)],
+            device_id={"sp": me + (1 if right else -1)},
+            device_id_type=MESH,
+        )
+
+    def kv_copy(slot, piece, right):
+        part = kv.at[slot, pl.ds(piece * CHUNK, CHUNK)]
+        return pltpu.make_async_remote_copy(
+            src_ref=part,
+            dst_ref=part,
+            send_sem=kv_send.at[slot, piece, int(right)],
+            recv_sem=kv_recv.at[slot, piece],
+            device_id={"sp": me + (1 if right else -1)},
+            device_id_type=MESH,
+        )
+
+    @pl.when(jnp.logical_not(has_left))
+    def _():
+        lkv[pl.ds(0, WINDOW), :] = jnp.zeros((WINDOW, 2 * HEAD), jnp.bfloat16)
+
+    @pl.when(jnp.logical_not(has_right))
+    def _():
+        lkv[pl.ds(WINDOW + rows, WINDOW), :] = jnp.zeros((WINDOW, 2 * HEAD), jnp.bfloat16)
 
     loads[0].wait()
     for i in range(1, 5):
@@ -140,60 +174,35 @@
         kv[me, pl.ds(at, CHUNK), HEAD:] = made[:, HEAD : 2 * HEAD]
         lkv[pl.ds(pl.multiple_of(WINDOW + at, WINDOW), CHUNK), :] = made[:, 2 * HEAD :]
 
-    kv_chunk(0)
-    loads[5].wait()
-
-    @pl.loop(1, chunks)
-    def _(c):
+    for step, c in enumerate(order):
+        if step == 1:
+            loads[5].wait()
         kv_chunk(c)
 
-    def halo_copy(right):
-        src, dst = (rows, 0) if right else (WINDOW, WINDOW + rows)
-        return pltpu.make_async_remote_copy(
-            src_ref=lkv.at[pl.ds(src, WINDOW)],
-            dst_ref=lkv.at[pl.ds(dst, WINDOW)],
-            send_sem=halo_send.at[int(right)],
-            recv_sem=halo_recv.at[int(right)],
-            device_id={"sp": me + (1 if right else -1)},
-            device_id_type=MESH,
-        )
-
-    def kv_copy(slot, to, sem):
-        return pltpu.make_async_remote_copy(
-            src_ref=kv.at[slot],
-            dst_ref=kv.at[slot],
-            send_sem=sem,
-            recv_sem=kv_recv.at[slot],
-            device_id={"sp": to},
-            device_id_type=MESH,
-        )
-
-    has_right = me < n_sp - 1
-    has_left = me > 0
-
-    @pl.when(has_right)
-    def _():
-        halo_copy(True).start()
-
-    @pl.when(has_left)
-    def _():
-        halo_copy(False).start()
-
-    @pl.when(jnp.logical_not(has_left))
-    def _():
-        lkv[pl.ds(0, WINDOW), :] = jnp.zeros((WINDOW, 2 * HEAD), jnp.bfloat16)
-
-    @pl.when(jnp.logical_not(has_right))
-    def _():
-        lkv[pl.ds(WINDOW + rows, WINDOW), :] = jnp.zeros((WINDOW, 2 * HEAD), jnp.bfloat16)
-
-    own_sends = ((1, 0), (-1, 1), (2, 2), (-2, 3))
-    for step, index in own_sends:
-        other = me + step
-
-        @pl.when((other >= 0) & (other < n_sp))
-        def _():
-            kv_copy(me, other, kv_send.at[index]).start()
+        @pl.when(has_right)
+        def _():
+            if c == chunks - 1:
+                halo_copy(True).start()
+            kv_copy(me, c, True).start()
+
+        @pl.when(has_left)
+        def _():
+            if c == 0:
+                halo_copy(False).start()
+            kv_copy(me, c, False).start()
+
+    def relay(k, piece):
+        for right in (True, False):
+            slot = me + k if right else me - k
+            here = (slot < n_sp) if right else (slot >= 0)
+
+            @pl.when(here)
+            def _():
+                kv_copy(slot, piece, not right).wait_recv()
+
+                @pl.when(has_left if right else has_right)
+                def _():
+                    kv_copy(slot, piece, not right).start()
 
     loads[6].wait()
     loads[7].wait()
@@ -234,6 +243,9 @@
     def _(u):
         attend(u, me, True)
 
+    for piece in order[:2]:
+        relay(1, piece)
+
     @pl.when(has_left)
     def _():
         halo_copy(True).wait_recv()
@@ -281,30 +293,29 @@
         alone = me + lean * (j - both)
         return jnp.where(j <= 2 * both, paired, alone)
 
-    def onward(slot):
-        away = slot - me
-        to = jnp.where(away > 0, me - 1, me + 1)
-        far = (away >= 2) | (away <= -2)
-        return to, far & (to >= 0) & (to < n_sp)
-
-    def arrive(j):
-        slot = block_of(j)
-        kv_copy(slot, jnp.where(has_left, me - 1, me + 1), fwd_send.at[slot]).wait_recv()
-        to, goes = onward(slot)
-
-        @pl.when(goes)
-        def _():
-            kv_copy(slot, to, fwd_send.at[slot]).start()
-
-        return slot
+    for piece in order[2:]:
+        relay(1, piece)
 
     @pl.loop(1, n_sp - 1)
     def _(j):
-        slot = arrive(j)
+        slot = block_of(j)
+        alone = j > 2 * both
+        k = jnp.where(alone, j - both, (j + 1) // 2)
+        first = alone | (lax.rem(j, 2) == 1)
+        final = alone | (lax.rem(j, 2) == 0)
 
         @pl.loop(0, units)
         def _(u):
             attend(u, slot, False)
+
+        @pl.when(first)
+        def _():
+            relay(k + 1, order[0])
+
+        @pl.when(final)
+        def _():
+            for piece in order[1:]:
+                relay(k + 1, piece)
 
     def pair_copy(u):
         return pltpu.make_async_remote_copy(
@@ -337,7 +348,7 @@
             sbuf[u, k - 1] = total.astype(jnp.bfloat16)
             chip_copy(u, k).start()
 
-    last = arrive(n_sp - 1)
+    last = block_of(n_sp - 1)
     loads[8].wait()
     loads[9].wait()
     tile = 512
@@ -382,21 +393,17 @@
     def _():
         halo_copy(False).wait_send()
 
-    for step, index in own_sends:
-        other = me + step
-
-        @pl.when((other >= 0) & (other < n_sp))
-        def _():
-            kv_copy(me, other, kv_send.at[index]).wait_send()
-
-    @pl.loop(1, n_sp)
-    def _(j):
-        slot = block_of(j)
-        to, goes = onward(slot)
-
-        @pl.when(goes)
-        def _():
-            kv_copy(slot, to, fwd_send.at[slot]).wait_send()
+    @pl.loop(0, n_sp)
+    def _(slot):
+        @pl.when((slot <= me) & has_right)
+        def _():
+            for piece in order:
+                kv_copy(slot, piece, True).wait_send()
+
+        @pl.when((slot >= me) & has_left)
+        def _():
+            for piece in order:
+                kv_copy(slot, piece, False).wait_send()
 
 
 def solution(mesh):
@@ -441,9 +448,8 @@
                 pltpu.VMEM((units, chips - 1, PIECE, width), bf16),
                 pltpu.VMEM((units, chips - 1, PIECE, width), bf16),
                 dma((10,)),
-                dma((n_sp,)),
-                dma((4,)),
-                dma((n_sp,)),
+                dma((n_sp, rows // CHUNK)),
+                dma((n_sp, rows // CHUNK, 2)),
                 dma((2,)),
                 dma((2,)),
                 dma((units,)),

time: 72.3 us -> 60.8 us (0.84)
  Pallas kernels: 70.3 us -> 58.9 us
    pallas_call x1, Pallas kernels: 70.3 us -> 58.9 us  [shards(): pl.pallas_call(functools.partial(kernel, n_sp, n_tp, rows, width), out_sh...]
where the time goes in v2:
time: 60.8 us; the launch traced here: 60.6 us
  Pallas kernels  58.9 us (97%)
  local copies, waits for them, and re-layouts  1.77 us (3%)
    pallas_call x1, Pallas kernels, shards(): pl.pallas_call(functools.partial(kernel, n_sp, n_tp, rows, width), out_sh...  58.9 us
    unnamed x1, local copies, waits for them, and re-layouts  1.77 us

profile of v2, /device:TPU:0, one launch (start us, length us, event | category | flops | bytes accessed | tf_op | source)
XLA Modules:
  0.0 60.6 jit_solution(17165000456472685377)
XLA Ops:
  0.0 58.9 %attention.1 = bf16[96,2048]{1,0:T(8,128)(2,1)} custom-call(bf16[768,2048]{1,0:T(8,128)(2,1)} %tokens.1, f32[1,2048]{1,0:T(1,128)} %bitcast.3, bf16[2048,256]{1,0:T(8,128)(2,1)} %gqw.1, bf16[2048,128]{1,0:T(8,128)(2,1)} %gkw.1, bf16[2048,128]{1,0:T(8,128)(2,1)} %gvw.1, f32[1,128]{1,0:T(1,128)} %bitcast.4, f32[1,128]{1,0:T(1,128)} %bitcast.5, ...), custom_call_target="tpu_custom_call" | custom-call | tf_op jit(solution)/shard_map/attention/pallas_call | solution.py:426
  58.9 1.8 %copy.17 = bf16[96,2048]{1,0:T(8,128)(2,1)} copy(bf16[96,2048]{1,0:T(8,128)(2,1)} %attention.1) | data formatting | bytes 786432

commit v3 on v2

--- a/solution.py
+++ b/solution.py
@@ -55,7 +55,7 @@
     n_sp, n_tp, rows, width,
     tokens, gain, gqw, gkw, gvw, gq_gain, gk_gain, lqw, lkw, lvw, sink, gow, low, row_tab, col_tab,
     out,
-    tok_v, normed, wkv, wq, wo, kv, lkv, q_s, lq_s, lo_s, acc, m_s, pbuf, rbuf0, sbuf, rbuf1,
+    tok_v, normed, wkv, wq, wo, kv, lkv, q_s, lq_s, lo_s, acc, m_s, pbuf, rbuf0, sbuf1, rbuf1, sbuf2, rbuf2,
     in_sem, kv_recv, kv_send, halo_recv, halo_send, r0_send, r0_recv, r1_send, r1_recv,
 ):
     me = lax.axis_index("sp")
@@ -67,6 +67,15 @@
     unit_rows = n_tp * PIECE
     partner = tp + 1 - 2 * par
 
+    def facing(k):
+        low_bit, high_bit = lax.rem(chip, 2), chip // 2
+        if k & 1:
+            low_bit = 1 - low_bit
+        if k & 2:
+            high_bit = 1 - high_bit
+        return high_bit * 2 + low_bit
+
+
     chunks = rows // CHUNK
     loads = []
 
@@ -93,11 +102,11 @@
             pl.semaphore_signal(barrier, inc=1, device_id={"sp": other}, device_id_type=MESH)
 
     pl.semaphore_signal(barrier, inc=1, device_id={"tp": partner}, device_id_type=MESH)
-    for k in range(1, chips):
-        peer = lax.rem(chip + k, chips) * 2 + par
-        pl.semaphore_signal(barrier, inc=1, device_id={"tp": peer}, device_id_type=MESH)
+    for k in (1, 2):
+        pl.semaphore_signal(
+            barrier, inc=1, device_id={"tp": facing(k) * 2 + par}, device_id_type=MESH
+        )
     near = jnp.minimum(me, 1) + jnp.minimum(n_sp - 1 - me, 1)
-    pl.semaphore_wait(barrier, near + chips)
 
     def norm_heads(x, head_gain):
         return x * lax.rsqrt(jnp.mean(x * x, axis=-1, keepdims=True) + EPSILON) * head_gain
@@ -178,6 +187,8 @@
         if step == 1:
             loads[5].wait()
         kv_chunk(c)
+        if step == 0:
+            pl.semaphore_wait(barrier, near + 3)
 
         @pl.when(has_right)
         def _():
@@ -327,26 +338,39 @@
             device_id_type=MESH,
         )
 
-    def chip_copy(u, k):
-        to = lax.rem(chip + k, chips)
+    half = width // 2
+    columns = (slice(0, half), slice(half, width))
+
+    def chip_copy(u, stage, way):
+        src, dst = (sbuf1, rbuf1) if stage == 0 else (sbuf2, rbuf2)
+        peer = facing(1 if stage == way else 2)
         return pltpu.make_async_remote_copy(
-            src_ref=sbuf.at[u, k - 1],
-            dst_ref=rbuf1.at[u, k - 1],
-            send_sem=r1_send.at[u, k - 1],
-            recv_sem=r1_recv.at[u, k - 1],
-            device_id={"tp": to * 2 + par},
+            src_ref=src.at[u, way],
+            dst_ref=dst.at[u, way],
+            send_sem=r1_send.at[u, stage, way],
+            recv_sem=r1_recv.at[u, stage, way],
+            device_id={"tp": peer * 2 + par},
             device_id_type=MESH,
         )
+
+    def paired(u, to, way):
+        return pbuf[u, par * chips + to, :, columns[way]].astype(jnp.float32) + rbuf0[
+            u, to, :, columns[way]
+        ].astype(jnp.float32)
 
     def spread(u):
         pair_copy(u).wait_recv()
-        for k in range(1, chips):
-            to = lax.rem(chip + k, chips)
-            total = pbuf[u, par * chips + to].astype(jnp.float32) + rbuf0[u, to].astype(
-                jnp.float32
-            )
-            sbuf[u, k - 1] = total.astype(jnp.bfloat16)
-            chip_copy(u, k).start()
+        for way in range(2):
+            sbuf1[u, way, 0] = paired(u, facing(1 + way), way).astype(jnp.bfloat16)
+            sbuf1[u, way, 1] = paired(u, facing(3), way).astype(jnp.bfloat16)
+            chip_copy(u, 0, way).start()
+
+    def pass_on(u):
+        for way in range(2):
+            chip_copy(u, 0, way).wait_recv()
+            total = paired(u, facing(2 - way), way) + rbuf1[u, way, 1].astype(jnp.float32)
+            sbuf2[u, way] = total.astype(jnp.bfloat16)
+            chip_copy(u, 1, way).start()
 
     last = block_of(n_sp - 1)
     loads[8].wait()
@@ -371,19 +395,23 @@
 
     @pl.loop(0, units)
     def _(u):
-        total = pbuf[u, par * chips + chip].astype(jnp.float32) + rbuf0[u, chip].astype(
-            jnp.float32
-        )
-        for k in range(1, chips):
-            chip_copy(u, k).wait_recv()
-            total = total + rbuf1[u, k - 1].astype(jnp.float32)
-        out[pl.ds(pl.multiple_of(u * PIECE, PIECE), PIECE), :] = total.astype(jnp.bfloat16)
+        pass_on(u)
+
+    @pl.loop(0, units)
+    def _(u):
+        at = pl.ds(pl.multiple_of(u * PIECE, PIECE), PIECE)
+        for way in range(2):
+            chip_copy(u, 1, way).wait_recv()
+            total = paired(u, chip, way) + rbuf1[u, way, 0].astype(jnp.float32)
+            total = total + rbuf2[u, way].astype(jnp.float32)
+            out[at, columns[way]] = total.astype(jnp.bfloat16)
 
     @pl.loop(0, units)
     def _(u):
         pair_copy(u).wait_send()
-        for k in range(1, chips):
-            chip_copy(u, k).wait_send()
+        for stage in range(2):
+            for way in range(2):
+                chip_copy(u, stage, way).wait_send()
 
     @pl.when(has_right)
     def _():
@@ -445,8 +473,10 @@
                 pltpu.VMEM((units, 2, unit_rows, HEAD), f32),
                 pltpu.VMEM((units, n_tp, PIECE, width), bf16),
                 pltpu.VMEM((units, chips, PIECE, width), bf16),
-                pltpu.VMEM((units, chips - 1, PIECE, width), bf16),
-                pltpu.VMEM((units, chips - 1, PIECE, width), bf16),
+                pltpu.VMEM((units, 2, 2, PIECE, width // 2), bf16),
+                pltpu.VMEM((units, 2, 2, PIECE, width // 2), bf16),
+                pltpu.VMEM((units, 2, PIECE, width // 2), bf16),
+                pltpu.VMEM((units, 2, PIECE, width // 2), bf16),
                 dma((10,)),
                 dma((n_sp, rows // CHUNK)),
                 dma((n_sp, rows // CHUNK, 2)),
@@ -454,8 +484,8 @@
                 dma((2,)),
                 dma((units,)),
                 dma((units,)),
-                dma((units, chips - 1)),
-                dma((units, chips - 1)),
+                dma((units, 2, 2)),
+                dma((units, 2, 2)),
             ],
             compiler_params=pltpu.CompilerParams(
                 collective_id=0, has_side_effects=True, vmem_limit_bytes=60 * 2**20

time: 60.8 us -> 56.7 us (0.933)
  Pallas kernels: 58.9 us -> 54.8 us
    pallas_call x1, Pallas kernels: 58.9 us -> 54.8 us  [shards(): pl.pallas_call(functools.partial(kernel, n_sp, n_tp, rows, width), out_sh...]
where the time goes in v3:
time: 56.7 us; the launch traced here: 56.5 us
  Pallas kernels  54.8 us (97%)
  local copies, waits for them, and re-layouts  1.77 us (3%)
    pallas_call x1, Pallas kernels, shards(): pl.pallas_call(functools.partial(kernel, n_sp, n_tp, rows, width), out_sh...  54.8 us
    unnamed x1, local copies, waits for them, and re-layouts  1.77 us

profile of v3, /device:TPU:0, one launch (start us, length us, event | category | flops | bytes accessed | tf_op | source)
XLA Modules:
  0.0 56.5 jit_solution(13128155546454375848)
XLA Ops:
  0.0 54.8 %attention.1 = bf16[96,2048]{1,0:T(8,128)(2,1)} custom-call(bf16[768,2048]{1,0:T(8,128)(2,1)} %tokens.1, f32[1,2048]{1,0:T(1,128)} %bitcast.3, bf16[2048,256]{1,0:T(8,128)(2,1)} %gqw.1, bf16[2048,128]{1,0:T(8,128)(2,1)} %gkw.1, bf16[2048,128]{1,0:T(8,128)(2,1)} %gvw.1, f32[1,128]{1,0:T(1,128)} %bitcast.4, f32[1,128]{1,0:T(1,128)} %bitcast.5, ...), custom_call_target="tpu_custom_call" | custom-call | tf_op jit(solution)/shard_map/attention/pallas_call | solution.py:454
  54.8 1.8 %copy.17 = bf16[96,2048]{1,0:T(8,128)(2,1)} copy(bf16[96,2048]{1,0:T(8,128)(2,1)} %attention.1) | data formatting | bytes 786432
